TPU v7x, 32 devices: a whole 2x2x4 slice. The times are simulated.
32 devices in a mesh: ep: 8 (over z, x), tp: 4 (over y, core).
Axes of the slice: x: 2, y: 2, z: 4, core: 2. Of those that a mesh axis runs over, the one named last changes fastest.
Arguments:
- queries: bfloat16 [2048, 1024], P('ep', 'tp'), may hold values from -6 to 6
- key_rows: bfloat16 [2048, 1024], P('ep', 'tp'), may hold values from -6 to 6
- value_rows: bfloat16 [2048, 1024], P('ep', 'tp'), may hold values from -6 to 6
- out_gate: bfloat16 [2048, 1024], P('ep', 'tp'), may hold values from -6 to 6
- log_decay: float32 [2048, 8], P('ep', 'tp'), may hold values from -3 to 0, as said below
- head_gain: float32 [8, 128], P('tp'), may hold values from 0.1 to 1.9
- out_weight: bfloat16 [1024, 2048], P('tp'), may hold values from -0.1875 to 0.1875
- moe_input: bfloat16 [1024, 2048], P('ep'), may hold values from -6 to 6
- moe_gain: float32 [2048], replicated, may hold values from 0.1 to 1.9
- expert_gate: bfloat16 [8, 2048, 3584], P('ep', None, 'tp'), may hold values from -0.125 to 0.125
- expert_up: bfloat16 [8, 2048, 3584], P('ep', None, 'tp'), may hold values from -0.125 to 0.125
- expert_down: bfloat16 [8, 3584, 2048], P('ep', 'tp'), may hold values from -0.125 to 0.125
- route_ids: int32 [1024, 2], P('ep'), may hold values from 0 to 7, all different within a row; in each aligned block of 128 rows (0 to 127, 128 to 255, ...) at most 64 rows name the same one
- route_weights: float32 [1024, 2], P('ep'), may hold values from 0.2 to 1
Outputs:
- mixer_out: bfloat16 [2048, 2048], P(('ep', 'tp'))
- expert_out: bfloat16 [1024, 2048], P('ep', 'tp')
Inputs may be any that keep to these rules, and one draw needn't show every extreme that they name: `route_ids`: among the 2 entries of a row no expert repeats. In each aligned block of 128 rows (the rows of one index of ep) no expert is named more than 64 times, a bound that some block reaches. `log_decay`: every entry is negative.
All inputs are finite; a program needn't handle non-finite values.
Results may differ from a plain program's by a relative error of at most 0.017.
Values may be sent and summed in bfloat16 or wider, within the bound.
A program may use at most 64 MiB of HBM per device.

v0:
```python
import jax
import jax.numpy as jnp
from jax import lax
from jax.sharding import PartitionSpec as P

TOP = 2


epsilon = 1e-06


def entering_2(x, axis, combine, identity):
    size, index = (lax.axis_size(axis), lax.axis_index(axis))
    everything = jax.tree.map(
        lambda part, kind: lax.all_gather(part.astype(kind), axis), x, (jnp.bfloat16, jnp.bfloat16)
    )
    start = jax.tree.map(
        lambda part, zero: jnp.broadcast_to(jnp.asarray(zero, part.dtype), part.shape), x, identity
    )

    def step(k, before):
        reached = k < index
        new = combine(
            before, jax.tree.map(lambda part, own: part[k].astype(own.dtype), everything, x)
        )
        return jax.tree.map(lambda a, b: jnp.where(reached, a, b), new, before)

    return lax.fori_loop(0, size, step, start)


def combine_states(earlier, later):
    return (earlier[0] + later[0], jnp.exp(later[0])[:, None, None] * earlier[1] + later[1])


def retention_half(queries, key_rows, value_rows, out_gate, log_decay, head_gain, out_weight):
    length = queries.shape[0]
    local_heads = log_decay.shape[1]
    head_dim = queries.shape[1] // local_heads
    query_heads = queries.reshape(length, local_heads, head_dim)
    key_heads = key_rows.reshape(length, local_heads, head_dim)
    value_heads = value_rows.reshape(length, local_heads, head_dim)
    cumulative = jnp.cumsum(log_decay, axis=0)
    block_total = cumulative[-1]
    scores = jnp.einsum(
        "thd,shd->hts", query_heads, key_heads, preferred_element_type=jnp.float32
    ) * head_dim ** (-0.5)
    level = cumulative.T
    causal = lax.broadcasted_iota(jnp.int32, (length, length), 0) >= lax.broadcasted_iota(
        jnp.int32, (length, length), 1
    )
    spread = jnp.where(causal[None], level[:, :, None] - level[:, None, :], -jnp.inf)
    weights = (scores * jnp.exp(spread)).astype(jnp.bfloat16)
    inner = jnp.einsum("hts,shd->thd", weights, value_heads, preferred_element_type=jnp.float32)
    value_f = value_heads.astype(jnp.float32)
    scaled_keys = (
        key_heads.astype(jnp.float32) * jnp.exp(block_total[None, :] - cumulative)[:, :, None]
    )
    local_state = jnp.einsum("thd,the->hde", scaled_keys, value_f, precision=lax.Precision.HIGHEST)
    identity = (jnp.zeros_like(block_total), jnp.zeros_like(local_state))
    _, entering = entering_2((block_total, local_state), "ep", combine_states, identity)
    scaled_queries = query_heads.astype(jnp.float32) * jnp.exp(cumulative)[:, :, None]
    carried = jnp.einsum("thd,hde->the", scaled_queries, entering, precision=lax.Precision.HIGHEST)
    retained = inner + carried
    normed = (
        retained
        * lax.rsqrt(jnp.mean(retained * retained, axis=-1, keepdims=True) + epsilon)
        * head_gain[None]
    )
    gated = normed * jax.nn.silu(
        out_gate.reshape(length, local_heads, head_dim).astype(jnp.float32)
    )
    heads_out = gated.reshape(length, local_heads * head_dim).astype(jnp.bfloat16)
    return lax.psum_scatter(
        jnp.dot(heads_out, out_weight, preferred_element_type=jnp.float32).astype(jnp.bfloat16),
        "tp",
        scatter_dimension=0,
        tiled=True,
    )


def pair_slots(route_ids, experts, capacity):
    flat_ids = route_ids.reshape(-1)
    member = (flat_ids[:, None] == jnp.arange(experts, dtype=jnp.int32)[None, :]).astype(jnp.int32)
    ranks = jnp.sum(jnp.cumsum(member, axis=0) * member, axis=1) - 1
    return flat_ids * capacity + ranks


def expert_half(moe_input, moe_gain, expert_gate, expert_up, expert_down, route_ids, route_weights):
    experts = lax.axis_size("ep")
    pairs = route_ids.size
    capacity = 2 * pairs // experts
    width = moe_input.shape[1]
    rows_f = moe_input.astype(jnp.float32)
    normed = (
        rows_f
        * lax.rsqrt(jnp.mean(rows_f * rows_f, axis=-1, keepdims=True) + epsilon)
        * moe_gain[None]
    ).astype(jnp.bfloat16)
    targets = pair_slots(route_ids, experts, capacity)
    table = (
        jnp.full((experts * capacity,), pairs, jnp.int32)
        .at[targets]
        .set(jnp.arange(pairs, dtype=jnp.int32))
    )
    filled = (table < pairs)[:, None]
    picked = jnp.where(
        filled, normed[jnp.minimum(table, pairs - 1) // TOP], jnp.zeros((), jnp.bfloat16)
    )
    outgoing = picked.reshape(experts, capacity, width)
    gate_slice = expert_gate[0]
    up_slice = expert_up[0]
    down_slice = expert_down[0]
    share = capacity // lax.axis_size("tp")
    piece = lax.dynamic_slice_in_dim(outgoing, lax.axis_index("tp") * share, share, 1)
    arrived = lax.all_to_all(piece, "ep", split_axis=0, concat_axis=0, tiled=True)
    rows = lax.all_gather(arrived, "tp", axis=1, tiled=True)
    gate_part = jnp.einsum("scd,df->scf", rows, gate_slice, preferred_element_type=jnp.float32)
    up_part = jnp.einsum("scd,df->scf", rows, up_slice, preferred_element_type=jnp.float32)
    hidden = (jax.nn.silu(gate_part) * up_part).astype(jnp.bfloat16)
    partial_sum = jnp.einsum("scf,fd->scd", hidden, down_slice, preferred_element_type=jnp.float32)
    reduced = lax.psum_scatter(
        partial_sum.astype(jnp.bfloat16), "tp", scatter_dimension=2, tiled=True
    )
    returned = lax.all_to_all(reduced, "ep", split_axis=0, concat_axis=0, tiled=True)
    columns = returned.shape[2]
    results = returned.reshape(experts * capacity, columns)[targets].astype(jnp.float32)
    results = results.reshape(pairs // TOP, TOP, columns)
    blended = jnp.sum(results * route_weights[:, :, None], axis=1)
    return blended.astype(jnp.bfloat16)


def per_device(
    queries,
    key_rows,
    value_rows,
    out_gate,
    log_decay,
    head_gain,
    out_weight,
    moe_input,
    moe_gain,
    expert_gate,
    expert_up,
    expert_down,
    route_ids,
    route_weights,
):
    mixer_out = retention_half(
        queries, key_rows, value_rows, out_gate, log_decay, head_gain, out_weight
    )
    expert_out = expert_half(
        moe_input, moe_gain, expert_gate, expert_up, expert_down, route_ids, route_weights
    )
    return (mixer_out, expert_out)


def solution(mesh):
    in_specs = (
        P("ep", "tp"),
        P("ep", "tp"),
        P("ep", "tp"),
        P("ep", "tp"),
        P("ep", "tp"),
        P("tp", None),
        P("tp", None),
        P("ep", None),
        P(),
        P("ep", None, "tp"),
        P("ep", None, "tp"),
        P("ep", "tp", None),
        P("ep", None),
        P("ep", None),
    )
    out_specs = (P(("ep", "tp"), None), P("ep", "tp"))
    return jax.shard_map(
        per_device, mesh=mesh, in_specs=in_specs, out_specs=out_specs, check_vma=False
    )
```

profile of v0, /device:TPU:0, one launch (start us, length us, event | category | flops | bytes accessed | tf_op | source)
XLA Modules:
  0.0 173.1 jit_solution(1716682732489076833)
XLA Ops:
  7.2 0.9 copy.85
  8.1 0.1 eq.29
  8.2 0.1 eq.25
  8.4 0.7 broadcast_multiply_fusion
  9.1 0.6 reduce-window.16
  9.6 0.2 slice_reduce_fusion
  10.0 0.1 copy.84
  10.1 0.1 mul.145
  10.3 1.4 scatter_custom_fusion
  11.8 1.2 fusion.15
  13.1 1.2 fusion.17
  14.4 3.3 %gather_fusion = bf16[512,2048]{1,0:T(8,128)(2,1)} fusion(bf16[128,2048]{1,0:T(8,128)(2,1)S(1)} %fusion.17, s32[1024]{0:T(1024)S(1)} %pad_clamp_fusion.1), kind=kCustom, calls=%fused_computation | custom fusion | bytes 4196352 | tf_op jit(solution)/shard_map/gather | solution.py:107
  17.7 1.3 dynamic-slice_select_fusion
  19.0 21.7 %all_to_all.10 = bf16[8,16,2048]{2,1,0:T(8,128)(2,1)} all-to-all(bf16[8,16,2048]{2,1,0:T(8,128)(2,1)S(1)} %dynamic-slice_select_fusion), channel_id=1, replica_groups=mesh['ep'=8,'tp'=4] {'ep'}, dimensions={0} | all-to-all | bytes 1048576 | tf_op jit(solution)/shard_map/all_to_all | solution.py:115
  40.8 0.6 reduce-window.14
  41.4 0.2 slice_reduce_fusion.1
  41.6 0.2 reduce-window.15
  41.9 0.2 fusion.50
  42.0 18.6 %all-gather.1 = bf16[8,1,2]{2,1,0:T(2,128)(2,1)S(1)} all-gather(bf16[1,1,2]{2,1,0:T(2,128)(2,1)S(1)} %bitcast.119), channel_id=1, replica_groups=mesh['ep'=8,'tp'=4] {'ep'}, dimensions={0}, use_global_device_ids=true | all-gather | bytes 36 | tf_op jit(solution)/shard_map/all_gather | solution.py:15
  60.6 0.1 copy.90
  60.7 0.1 copy.77
  60.8 0.1 copy.83
  60.9 0.2 slice_reduce_fusion.2
  61.2 0.3 convolution_convert_fusion.1
  61.5 31.5 %all-gather = bf16[16,128,128]{2,1,0:T(8,128)(2,1)S(1)} all-gather(bf16[2,128,128]{2,1,0:T(8,128)(2,1)S(1)} %convolution_convert_fusion.1), channel_id=2, replica_groups=mesh['ep'=8,'tp'=4] {'ep'}, dimensions={0}, use_global_device_ids=true | all-gather | bytes 589824 | tf_op jit(solution)/shard_map/all_gather | solution.py:15
  93.0 0.4 convolution_bitcast_fusion.1
  93.5 6.3 %fusion.5 = f32[8,64,896]{2,1,0:T(8,128)} fusion(bf16[8,64,2048]{2,1,0:T(8,128)(2,1)} %all-gather.4.cloned.1.call-done, bf16[1,2048,896]{2,1,0:T(8,128)(2,1)} %param.25), kind=kOutput, calls=%fused_computation.11 | convolution fusion | flops 1879048192 | bytes 7602176 | tf_op jit(solution)/shard_map/scd,df->scf/dot_general | solution.py:117
  99.8 10.2 %fusion.7 = bf16[8,64,2048]{2,1,0:T(8,128)(2,1)} fusion(bf16[1,896,2048]{2,1,0:T(8,128)(2,1)} %param.27, f32[8,64,896]{2,1,0:T(8,128)} %fusion.5, bf16[8,64,2048]{2,1,0:T(8,128)(2,1)} %all-gather.4.cloned.1.call-done, bf16[1,2048,896]{2,1,0:T(8,128)(2,1)} %param.26), kind=kOutput, calls=%fused_computation.13 | convolution fusion | flops 3761897472 | bytes 13369344 | tf_op jit(solution)/shard_map/scf,fd->scd/dot_general | solution.py:120
  110.0 2.5 %while.14 = (s32[]{:T(128)}, f32[2,128,128]{2,1,0:T(8,128)S(1)}, s32[]{:T(128)}, bf16[8,2]{0,1:T(2,128)(2,1)S(1)}, bf16[8,2,128,128]{3,2,1,0:T(8,128)(2,1)S(1)}, /*index=5*/s32[]{:T(128)}, s32[]{:T(128)}) while((s32[]{:T(128)}, f32[2,128,128]{2,1,0:T(8,128)S(1)}, s32[]{:T(128)}, bf16[8,2]{0,1:T(2,128)(2,1)S(1)}, ...), condition=%wide.region_3.4_spmd.clone, body=%wide.region_2.3_spmd.clone.sunk | while | flops 163846 | bytes 327821 | solution.py:28
  110.1 0.1 copy.122
  110.4 0.1 copy.122
  110.7 0.1 copy.122
  111.0 0.1 copy.122
  111.3 0.1 copy.122
  111.6 0.1 copy.122
  111.9 0.1 copy.122
  112.2 0.1 copy.122
  112.5 0.5 multiply_reduce_fusion.1
  113.0 0.1 multiply_convert_fusion.1
  113.2 1.4 convolution_convert_fusion
  114.6 24.0 %reduce-scatter.5.cloned.1.call-done = bf16[8,64,512]{2,1,0:T(8,128)(2,1)} async-done(((bf16[8,64,2048]{2,1,0:T(8,128)(2,1)}), bf16[8,64,512]{2,1,0:T(8,128)(2,1)}) %reduce-scatter.5.cloned.1.call-update) | async-done | bytes 524304 | tf_op jit(solution)/shard_map/reduce_scatter | solution.py:121
  138.7 5.5 %all-to-all-start.1 = ((bf16[8,64,512]{2,1,0:T(8,128)(2,1)}), bf16[8,64,512]{2,1,0:T(8,128)(2,1)S(1)}, u32[]{:S(2)}, u32[]{:S(2)}) async-start(bf16[8,64,512]{2,1,0:T(8,128)(2,1)} %reduce-scatter.5.cloned.1.call-done), calls=%async_computation.3 | async-start | bytes 1048576 | tf_op jit(solution)/shard_map/all_to_all | solution.py:124
  144.2 0.1 copy.87
  144.3 14.2 %all-to-all-done.1 = bf16[8,64,512]{2,1,0:T(8,128)(2,1)S(1)} async-done(((bf16[8,64,512]{2,1,0:T(8,128)(2,1)}), bf16[8,64,512]{2,1,0:T(8,128)(2,1)S(1)}, u32[]{:S(2)}, u32[]{:S(2)}) %all-to-all-start.1) | async-done | bytes 524320 | tf_op jit(solution)/shard_map/all_to_all | solution.py:124
  158.5 1.2 gather_fusion.1
  159.7 0.3 reshape.164
  160.0 1.4 multiply_reduce_fusion
  161.4 5.2 %reduce-scatter.3.cloned.1.call-done = bf16[64,2048]{1,0:T(8,128)(2,1)} async-done(((bf16[256,2048]{1,0:T(8,128)(2,1)}), bf16[64,2048]{1,0:T(8,128)(2,1)}) %reduce-scatter.3.cloned.1.call-update) | async-done | bytes 262160 | tf_op jit(solution)/shard_map/reduce_scatter | solution.py:73
  (68 shorter events, 2.2 us)
Async XLA Ops:
  7.2 106.0 %copy-start = (bf16[256,2048]{1,0:T(8,128)(2,1)S(1)}, bf16[256,2048]{1,0:T(8,128)(2,1)}, u32[]{:S(2)}) copy-start(bf16[256,2048]{1,0:T(8,128)(2,1)} %param.22) | copy-start | bytes 3145732
  7.2 86.3 %all-gather.4.cloned.1.call-start = ((), (), s32[]{:S(2)}) async-start(), calls=%async_computation.5 | async-start | bytes 2621440 | tf_op jit(solution)/shard_map/all_gather | solution.py:116
  17.7 23.1 %copy-start.5 = (f32[256,2]{0,1:T(2,128)S(1)}, f32[256,2]{0,1:T(2,128)}, u32[]{:S(2)}) copy-start(f32[256,2]{0,1:T(2,128)} %param.20) | copy-start | bytes 6148
  17.7 42.9 %copy-start.2 = (bf16[256,256]{1,0:T(8,128)(2,1)S(1)}, bf16[256,256]{1,0:T(8,128)(2,1)}, u32[]{:S(2)}) copy-start(bf16[256,256]{1,0:T(8,128)(2,1)} %param.17) | copy-start | bytes 393220
  17.7 43.1 %copy-start.1 = (bf16[256,256]{1,0:T(8,128)(2,1)S(1)}, bf16[256,256]{1,0:T(8,128)(2,1)}, u32[]{:S(2)}) copy-start(bf16[256,256]{1,0:T(8,128)(2,1)} %param.19) | copy-start | bytes 393220
  17.7 43.5 %copy-start.3 = (bf16[256,256]{1,0:T(8,128)(2,1)S(1)}, bf16[256,256]{1,0:T(8,128)(2,1)}, u32[]{:S(2)}) copy-start(bf16[256,256]{1,0:T(8,128)(2,1)} %param.18) | copy-start | bytes 393220
  17.7 75.3 %copy-start.4 = (bf16[256,256]{1,0:T(8,128)(2,1)S(1)}, bf16[256,256]{1,0:T(8,128)(2,1)}, u32[]{:S(2)}) copy-start(bf16[256,256]{1,0:T(8,128)(2,1)} %param.16) | copy-start | bytes 393220
  40.7 97.9 %reduce-scatter.5.cloned.1.call-start = ((), (), s32[]{:S(2)}) async-start(), calls=%async_computation.6 | async-start | bytes 2621440 | tf_op jit(solution)/shard_map/reduce_scatter | solution.py:121
  109.9 3.1 %copy-start.6 = (f32[2,128]{1,0:T(2,128)S(1)}, f32[2,128]{1,0:T(2,128)}, u32[]{:S(2)}) copy-start(f32[2,128]{1,0:T(2,128)} %param.21) | copy-start | bytes 3076
  110.0 56.6 %reduce-scatter.3.cloned.1.call-start = ((), (), s32[]{:S(2)}) async-start(), calls=%async_computation.4 | async-start | bytes 1310720 | tf_op jit(solution)/shard_map/reduce_scatter | solution.py:73
  113.2 31.0 %copy-start.7 = (f32[128,2]{0,1:T(2,128)S(1)}, f32[128,2]{0,1:T(2,128)}, u32[]{:S(2)}) copy-start(f32[128,2]{0,1:T(2,128)} %param.29) | copy-start | bytes 3076
  138.7 19.9 %all-to-all-start.1 = ((bf16[8,64,512]{2,1,0:T(8,128)(2,1)}), bf16[8,64,512]{2,1,0:T(8,128)(2,1)S(1)}, u32[]{:S(2)}, u32[]{:S(2)}) async-start(bf16[8,64,512]{2,1,0:T(8,128)(2,1)} %reduce-scatter.5.cloned.1.call-done), calls=%async_computation.3 | async-start | bytes 1048576 | tf_op jit(solution)/shard_map/all_to_all | solution.py:124
Sparse Core Ops, SparseCore 0:
  40.9 21.5 all-gather.3
  110.1 28.5 reduce-scatter.4
  141.8 24.7 reduce-scatter.2
where the time goes:
time: 173 us
  blocking collectives  71.8 us (42%)
  waiting for transfers between devices  43.5 us (25%)
  matrix products  19.1 us (11%)
  between operations  14 us (8%)
  local copies, waits for them, and re-layouts  10.5 us (6%)
  other arithmetic  8.42 us (5%)
  starting transfers between devices  5.65 us (3%)
    all_gather x2, blocking collectives, entering_2(): lax.all_gather(part.astype(kind), axis)  50.1 us
    reduce_scatter x1, waiting for transfers between devices, expert_half(): lax.psum_scatter(partial_sum.astype(jnp.bfloat16), 'tp', scatter_dimensio...  24 us
    all_to_all x1, blocking collectives, expert_half(): lax.all_to_all(piece, 'ep', split_axis=0, concat_axis=0, tiled=True)  21.7 us
    all_to_all x1, waiting for transfers between devices, expert_half(): lax.all_to_all(reduced, 'ep', split_axis=0, concat_axis=0, tiled=True)  14.2 us
    dot_general x1, matrix products, expert_half(): jnp.einsum('scf,fd->scd', hidden, down_slice, preferred_element_type=jnp....  10.2 us
    dot_general x1, matrix products, expert_half(): jnp.einsum('scd,df->scf', rows, gate_slice, preferred_element_type=jnp.fl...  6.27 us
    all_to_all x1, starting transfers between devices, expert_half(): lax.all_to_all(reduced, 'ep', split_axis=0, concat_axis=0, tiled=True)  5.53 us
    reduce_scatter x1, waiting for transfers between devices, retention_half(): lax.psum_scatter(jnp.dot(heads_out, out_weight, preferred_element_type=jn...  5.22 us
  transfers between devices with their start and end apart: 4, of which 3 were waited for; matrix products, arithmetic and copies ran while one was open for 6% of the time, Pallas kernels for 0%

commit v1 on v0

v1 whole, which is shorter than its diff:
```python
import functools

import jax
import jax.numpy as jnp
from jax import lax
from jax.experimental import pallas as pl
from jax.experimental.pallas import tpu as pltpu
from jax.sharding import PartitionSpec as P

epsilon = 1e-06
CHUNKS = 2
BF = jnp.bfloat16
F32 = jnp.float32


def dot(a, b, dims=(((1,), (0,)), ((), ()))):
    return lax.dot_general(a, b, dims, preferred_element_type=F32)


def layer_kernel(
    n, cap, heads,
    q_ref, k_ref, v_ref, g_ref, cum_ref, cum_t_ref, gain_ref, piece_ref, hi_ref, lo_ref,
    ow_hbm, wg_hbm, wu_hbm, wd_hbm,
    mixer_ref, expert_ref,
    ow, wg, wu, wd, x, part, near, half, far, done, back,
    st, st_in, tot, tot_in, inner, ho, mx, mr1, ms, mr2,
    w_sem, own_sem, disp_s, disp_r, st_s, st_r, tot_s, tot_r, fwd_s, fwd_r,
    red_s, red_r, mix_s, mix_r, ret_s, ret_r,
):
    i, j = lax.axis_index("ep"), lax.axis_index("tp")
    j1 = j + 1 - 2 * lax.rem(j, 2)
    j2 = lax.rem(j + 2, 4)
    j3 = lax.rem(j1 + 2, 4)
    places = (j, j1, j2, j3)
    rows = n * cap
    step = rows // CHUNKS
    width = x.shape[2]
    dim = gain_ref.shape[1]
    length = q_ref.shape[0]
    quarter = length // 4

    def ahead(d):
        return lax.rem(i + d, n)

    def behind(d):
        return lax.rem(i + n - d, n)

    def send(src, dst, ss, rs, dev):
        return pltpu.make_async_remote_copy(
            src_ref=src, dst_ref=dst, send_sem=ss, recv_sem=rs, device_id=dev,
            device_id_type=pl.DeviceIdType.MESH,
        )

    loads = [
        pltpu.make_async_copy(a, b, w_sem.at[m])
        for m, (a, b) in enumerate(((ow_hbm, ow), (wg_hbm, wg), (wu_hbm, wu), (wd_hbm, wd)))
    ]
    for c in loads:
        c.start()
    own = pltpu.make_async_copy(piece_ref.at[pl.ds(0, cap)], x.at[0, pl.ds(0, cap)], own_sem.at[0])
    own.start()

    barrier = pltpu.get_barrier_semaphore()
    for d in range(1, n):
        pl.semaphore_signal(barrier, inc=1, device_id=(ahead(d), j), device_id_type=pl.DeviceIdType.MESH)
    for peer in (j1, j2):
        pl.semaphore_signal(barrier, inc=1, device_id=(i, peer), device_id_type=pl.DeviceIdType.MESH)
    pl.semaphore_wait(barrier, n + 1)

    sent = []
    disp = [None] * n
    for d in range(1, n):
        r = pl.ds(d * cap, cap)
        disp[d] = send(piece_ref.at[r], x.at[0, r], disp_s.at[d], disp_r.at[d], (ahead(d), j))
        disp[d].start()
        sent.append(disp[d])

    tot[...] = jnp.zeros_like(tot)
    for h in range(heads):
        c = slice(h * dim, (h + 1) * dim)
        total = cum_ref[length - 1 : length, h : h + 1]
        keys = k_ref[:, c].astype(F32) * jnp.exp(total - cum_ref[:, h : h + 1])
        st[h * dim : (h + 1) * dim, :] = dot(keys.T.astype(BF), v_ref[:, c]).astype(BF)
        tot[h : h + 1, :] = jnp.broadcast_to(total, (1, dim))
    st_c, tot_c = [None] * n, [None] * n
    for d in range(1, n):
        st_c[d] = send(st, st_in.at[d], st_s.at[d], st_r.at[d], (ahead(d), j))
        tot_c[d] = send(tot, tot_in.at[d], tot_s.at[d], tot_r.at[d], (ahead(d), j))

        @pl.when(i + d < n)
        def _():
            st_c[d].start()
            tot_c[d].start()

    y_c, c0_c, c2_c = [], [], []
    for g in range(CHUNKS):
        r = pl.ds(g * step, step)
        y_c.append(send(x.at[0, r], x.at[2, r], fwd_s.at[g, 0], fwd_r.at[g, 0], (i, j2)))
        c0_c.append(send(x.at[0, r], x.at[1, r], fwd_s.at[g, 1], fwd_r.at[g, 1], (i, j1)))
        c2_c.append(send(x.at[2, r], x.at[3, r], fwd_s.at[g, 2], fwd_r.at[g, 2], (i, j1)))
    sent += y_c + c0_c + c2_c

    def forward(g):
        for d in range(g * (n // CHUNKS), (g + 1) * (n // CHUNKS)):
            if d == 0:
                own.wait()
            else:
                disp[d].wait_recv()
        y_c[g].start()
        c0_c[g].start()

    def relay(g):
        y_c[g].wait_recv()
        c2_c[g].start()

    forward(0)

    causal = lax.broadcasted_iota(jnp.int32, (length, length), 0) >= lax.broadcasted_iota(
        jnp.int32, (length, length), 1
    )
    for h in range(heads):
        c = slice(h * dim, (h + 1) * dim)
        scores = dot(q_ref[:, c], k_ref[:, c], (((1,), (1,)), ((), ()))) * dim ** (-0.5)
        spread = jnp.where(causal, cum_ref[:, h : h + 1] - cum_t_ref[h : h + 1, :], -jnp.inf)
        inner[:, c] = dot((scores * jnp.exp(spread)).astype(BF), v_ref[:, c])

    for g in range(1, CHUNKS):
        forward(g)
    relay(0)

    entering = jnp.zeros((heads * dim, dim), F32)
    for d in range(n - 1, 0, -1):
        @pl.when(i >= d)
        def _():
            st_c[d].wait_recv()
            tot_c[d].wait_recv()

        @pl.when(i < d)
        def _():
            st_in[d] = jnp.zeros(st_in.shape[1:], BF)
            tot_in[d] = jnp.zeros(tot_in.shape[1:], F32)

        decay = jnp.concatenate(
            [jnp.broadcast_to(jnp.exp(tot_in[d, h : h + 1, :]), (dim, dim)) for h in range(heads)], axis=0
        )
        entering = decay * entering + st_in[d].astype(F32)
    entering = entering.astype(BF)
    for h in range(heads):
        c = slice(h * dim, (h + 1) * dim)
        queries = (q_ref[:, c].astype(F32) * jnp.exp(cum_ref[:, h : h + 1])).astype(BF)
        kept = inner[:, c] + dot(queries, entering[h * dim : (h + 1) * dim, :])
        normed = kept * lax.rsqrt(jnp.mean(kept * kept, axis=-1, keepdims=True) + epsilon)
        ho[:, c] = (normed * gain_ref[h : h + 1, :] * jax.nn.silu(g_ref[:, c].astype(F32))).astype(BF)
    loads[0].wait()
    mx[...] = dot(ho[...], ow[...]).astype(BF)

    def stripe(m):
        return pl.ds(pl.multiple_of(places[m] * quarter, quarter), quarter)

    mix_a = send(mx.at[stripe(1)], mr1.at[0], mix_s.at[0], mix_r.at[0], (i, j1))
    mix_b = send(mx.at[stripe(3)], mr1.at[1], mix_s.at[1], mix_r.at[1], (i, j1))
    mix_c = send(ms, mr2, mix_s.at[2], mix_r.at[2], (i, j2))
    mix_b.start()
    mix_a.start()
    sent += [mix_a, mix_b, mix_c]
    for g in range(1, CHUNKS):
        relay(g)
    for c in loads[1:]:
        c.wait()

    red = []
    for g in range(CHUNKS):
        r = pl.ds(g * step, step)
        red.append((
            send(part.at[1, r], near.at[0, r], red_s.at[g, 0], red_r.at[g, 0], (i, j1)),
            send(part.at[3, r], near.at[1, r], red_s.at[g, 1], red_r.at[g, 1], (i, j1)),
            send(half.at[r], far.at[r], red_s.at[g, 2], red_r.at[g, 2], (i, j2)),
        ))
        sent += list(red[-1])

    def block(m):
        return pl.ds(pl.multiple_of(places[m] * width, width), width)

    def experts(g):
        r = pl.ds(g * step, step)
        gate, up = 0.0, 0.0
        for m in (0, 2, 1, 3):
            if m == 1:
                c0_c[g].wait_recv()
                c2_c[g].wait_recv()
            gate = gate + dot(x[m, r, :], wg[block(m), :])
            up = up + dot(x[m, r, :], wu[block(m), :])
        hidden = (jax.nn.silu(gate) * up).astype(BF)
        for m in (3, 1, 2, 0):
            part[m, r, :] = dot(hidden, wd[:, block(m)]).astype(BF)
            if m == 3:
                red[g][1].start()
            if m == 1:
                red[g][0].start()

    def cross(g):
        r = pl.ds(g * step, step)
        red[g][1].wait_recv()
        half[r, :] = (part[2, r, :].astype(F32) + near[1, r, :].astype(F32)).astype(BF)
        red[g][2].start()

    ret = [None] * n
    for d in range(n):
        r = pl.ds(d * cap, cap)
        if d:
            ret[d] = send(done.at[r], back.at[r], ret_s.at[d], ret_r.at[d], (behind(d), j))
            sent.append(ret[d])

    def home(g):
        r = pl.ds(g * step, step)
        red[g][0].wait_recv()
        red[g][2].wait_recv()
        done[r, :] = (
            part[0, r, :].astype(F32) + near[0, r, :].astype(F32) + far[r, :].astype(F32)
        ).astype(BF)
        for d in range(g * (n // CHUNKS), (g + 1) * (n // CHUNKS)):
            if d:
                ret[d].start()
        if g == 0:
            back[pl.ds(0, cap), :] = done[pl.ds(0, cap), :]

    experts(0)
    cross(0)
    mix_b.wait_recv()
    ms[...] = (mx[stripe(2), :].astype(F32) + mr1[1].astype(F32)).astype(BF)
    mix_c.start()
    for g in range(1, CHUNKS):
        experts(g)
        home(g - 1)
        cross(g)
    mix_a.wait_recv()
    mix_c.wait_recv()
    mixer_ref[...] = (
        mx[stripe(0), :].astype(F32) + mr1[0].astype(F32) + mr2[...].astype(F32)
    ).astype(BF)
    home(CHUNKS - 1)
    for d in range(1, n):
        ret[d].wait_recv()
    expert_ref[...] = (dot(hi_ref[...], back[...]) + dot(lo_ref[...], back[...])).astype(BF)
    for c in sent:
        c.wait_send()
    for d in range(1, n):
        @pl.when(i + d < n)
        def _():
            st_c[d].wait_send()
            tot_c[d].wait_send()


def per_device(
    queries, key_rows, value_rows, out_gate, log_decay, head_gain, out_weight,
    moe_input, moe_gain, expert_gate, expert_up, expert_down, route_ids, route_weights,
):
    n, shares = lax.axis_size("ep"), lax.axis_size("tp")
    i, j = lax.axis_index("ep"), lax.axis_index("tp")
    tokens, top = route_ids.shape
    pairs = tokens * top
    cap = -(-2 * pairs // n // 16) * 16
    full = moe_input.shape[1]
    width = full // shares
    length, heads = log_decay.shape
    dim = head_gain.shape[1]
    hidden = expert_gate.shape[2]

    rows_f = moe_input.astype(F32)
    scale = lax.rsqrt(jnp.mean(rows_f * rows_f, axis=-1, keepdims=True) + epsilon)
    mine = lax.dynamic_slice_in_dim(moe_input, j * width, width, 1).astype(F32)
    gain = lax.dynamic_slice_in_dim(moe_gain, j * width, width, 0)
    normed = (mine * scale * gain[None]).astype(BF)

    flat = route_ids.reshape(-1)
    member = flat[:, None] == jnp.arange(n, dtype=jnp.int32)[None, :]
    lower = jnp.arange(pairs)[:, None] >= jnp.arange(pairs)[None, :]
    counts = jnp.dot(lower.astype(BF), member.astype(BF), preferred_element_type=F32)
    ranks = jnp.sum(jnp.where(member, counts, 0.0), axis=1).astype(jnp.int32) - 1
    targets = (lax.rem(flat - i + n, n) * cap + ranks).reshape(tokens, top)
    slots = jnp.arange(n * cap, dtype=jnp.int32)
    pick = sum(((targets[:, t][None, :] == slots[:, None]).astype(BF) for t in range(top)))
    piece = jnp.dot(pick, normed, preferred_element_type=F32).astype(BF)
    comb = sum(
        jnp.where(targets[:, t][:, None] == slots[None, :], route_weights[:, t][:, None], 0.0)
        for t in range(top)
    )
    hi = lax.reduce_precision(comb, 8, 7)
    lo = (comb - hi).astype(BF)
    hi = hi.astype(BF)
    cum = jnp.cumsum(log_decay, axis=0)

    rows = n * cap
    quarter = length // shares
    vmem = pl.BlockSpec(memory_space=pltpu.VMEM)
    hbm = pl.BlockSpec(memory_space=pl.ANY)
    dma = pltpu.SemaphoreType.DMA
    return pl.pallas_call(
        functools.partial(layer_kernel, n, cap, heads),
        out_shape=(
            jax.ShapeDtypeStruct((quarter, full), BF),
            jax.ShapeDtypeStruct((tokens, width), BF),
        ),
        in_specs=[vmem] * 10 + [hbm] * 4,
        out_specs=(vmem, vmem),
        scratch_shapes=[
            pltpu.VMEM(out_weight.shape, BF),
            pltpu.VMEM((full, hidden), BF),
            pltpu.VMEM((full, hidden), BF),
            pltpu.VMEM((hidden, full), BF),
            pltpu.VMEM((4, rows, width), BF),
            pltpu.VMEM((4, rows, width), BF),
            pltpu.VMEM((2, rows, width), BF),
            pltpu.VMEM((rows, width), BF),
            pltpu.VMEM((rows, width), BF),
            pltpu.VMEM((rows, width), BF),
            pltpu.VMEM((rows, width), BF),
            pltpu.VMEM((heads * dim, dim), BF),
            pltpu.VMEM((n, heads * dim, dim), BF),
            pltpu.VMEM((8, dim), F32),
            pltpu.VMEM((n, 8, dim), F32),
            pltpu.VMEM((length, heads * dim), F32),
            pltpu.VMEM((length, heads * dim), BF),
            pltpu.VMEM((length, full), BF),
            pltpu.VMEM((2, quarter, full), BF),
            pltpu.VMEM((quarter, full), BF),
            pltpu.VMEM((quarter, full), BF),
            dma((4,)), dma((1,)),
            dma((n,)), dma((n,)), dma((n,)), dma((n,)), dma((n,)), dma((n,)),
            dma((CHUNKS, 3)), dma((CHUNKS, 3)),
            dma((CHUNKS, 3)), dma((CHUNKS, 3)),
            dma((3,)), dma((3,)),
            dma((n,)), dma((n,)),
        ],
        compiler_params=pltpu.CompilerParams(
            collective_id=0, has_side_effects=True, vmem_limit_bytes=60 * 1024 * 1024
        ),
    )(
        queries, key_rows, value_rows, out_gate, cum, cum.T, head_gain, piece, hi, lo,
        out_weight, expert_gate[0], expert_up[0], expert_down[0],
    )


def solution(mesh):
    in_specs = (
        P("ep", "tp"),
        P("ep", "tp"),
        P("ep", "tp"),
        P("ep", "tp"),
        P("ep", "tp"),
        P("tp", None),
        P("tp", None),
        P("ep", None),
        P(),
        P("ep", None, "tp"),
        P("ep", None, "tp"),
        P("ep", "tp", None),
        P("ep", None),
        P("ep", None),
    )
    out_specs = (P(("ep", "tp"), None), P("ep", "tp"))
    return jax.shard_map(
        per_device, mesh=mesh, in_specs=in_specs, out_specs=out_specs, check_vma=False
    )
```

time: 173 us -> 82.3 us (0.48)
  blocking collectives: 71.8 us -> 0 us
  Pallas kernels: 0 us -> 67.8 us
  waiting for transfers between devices: 43.5 us -> 0 us
  matrix products: 19.1 us -> 2.26 us
  between operations: 14 us -> 0.68 us
  starting transfers between devices: 5.65 us -> 0 us
  other arithmetic: 8.42 us -> 3.67 us
  local copies, waits for them, and re-layouts: 10.5 us -> 7.55 us
    pallas_call x0 -> x1, Pallas kernels: none -> 67.8 us  [per_device(): pl.pallas_call(functools.partial(layer_kernel, n, cap, heads), out_shape=...]
    all_gather x2 -> x0, blocking collectives: 50.1 us -> none  [entering_2(): lax.all_gather(part.astype(kind), axis)]
    reduce_scatter x2 -> x0, waiting for transfers between devices: 29.2 us -> none  [the longest x1 24 us: expert_half(): lax.psum_scatter(partial_sum.astype(jnp.bfloat16), 'tp', scatter_dimensio...]
    all_to_all x1 -> x0, blocking collectives: 21.7 us -> none  [expert_half(): lax.all_to_all(piece, 'ep', split_axis=0, concat_axis=0, tiled=True)]
    dot_general x6 -> x2, matrix products: 19.1 us -> 2.26 us  [the longest x1 2.06 us: per_device(): piece = jnp.dot(pick, normed, preferred_element_type=F32).astype(BF)]
    all_to_all x1 -> x0, waiting for transfers between devices: 14.2 us -> none  [expert_half(): lax.all_to_all(reduced, 'ep', split_axis=0, concat_axis=0, tiled=True)]
    all_to_all x1 -> x0, starting transfers between devices: 5.53 us -> none  [expert_half(): lax.all_to_all(reduced, 'ep', split_axis=0, concat_axis=0, tiled=True)]
    gather x2 -> x0, local copies, waits for them, and re-layouts: 4.5 us -> none  [the longest x1 3.35 us: expert_half(): normed[jnp.minimum(table, pairs - 1) // TOP]]
  transfers between devices with their start and end apart: 4 -> 0, of which waited for: 3 -> 0; matrix products, arithmetic and copies ran while one was open for 6% -> 0% of each run, Pallas kernels for 0% -> 0%
where the time goes in v1:
time: 82.3 us; the launch traced here: 82 us
  Pallas kernels  67.8 us (82%)
  local copies, waits for them, and re-layouts  7.55 us (9%)
  other arithmetic  3.67 us (4%)
  matrix products  2.26 us (3%)
    pallas_call x1, Pallas kernels, per_device(): pl.pallas_call(functools.partial(layer_kernel, n, cap, heads), out_shape=...  67.8 us
    unnamed x6, local copies, waits for them, and re-layouts  4.03 us
    dot_general x1, matrix products, per_device(): piece = jnp.dot(pick, normed, preferred_element_type=F32).astype(BF)  2.06 us

profile of v1, /device:TPU:0, one launch (start us, length us, event | category | flops | bytes accessed | tf_op | source)
XLA Modules:
  0.0 82.0 jit_solution(368548431029150079)
XLA Ops:
  0.6 1.2 %multiply_reduce_fusion = f32[128]{0:T(128)S(1)} fusion(bf16[128,2048]{1,0:T(8,128)(2,1)} %param.21), kind=kLoop, calls=%fused_computation.3 | loop fusion | flops 786304 | bytes 524800 | tf_op jit(solution)/shard_map/reduce_sum | solution.py:270
  1.9 0.8 slice_bitcast_fusion.1
  2.6 0.7 reshape.32
  3.3 0.6 reduce-window.6
  3.9 0.2 slice_reduce_fusion
  4.1 0.2 reduce-window.9
  4.3 0.1 add_bitcast_fusion
  4.4 0.0 copy-start
  4.4 0.8 dynamic_slice.7
  5.1 0.8 copy.35
  5.9 0.1 eq.71
  6.0 0.2 fusion
  6.3 0.1 sub.19
  6.4 0.1 copy.36
  6.5 0.7 fusion.15
  7.2 0.8 copy.37.cum_ref
  8.0 0.9 %fusion.1 = (bf16[128,512]{1,0:T(8,128)(2,1)}, bf16[128,512]{1,0:T(8,128)(2,1)}) fusion(f32[128]{0:T(128)S(1)} %get-tuple-element.7, s32[128]{0:T(128)S(1)} %get-tuple-element.9, f32[128]{0:T(128)S(1)} %get-tuple-element.6, s32[128]{0:T(128)S(1)} %get-tuple-element.8), kind=kLoop, calls=%fused_computation.6 | loop fusion | flops 589824 | bytes 264192 | tf_op jit(solution)/shard_map/convert_element_type | solution.py:289
  8.8 2.1 %convolution_convert_fusion.piece_ref = bf16[512,512]{1,0:T(8,128)(2,1)} fusion(f32[512]{0:T(512)S(1)} %dynamic_slice.7, f32[128]{0:T(128)S(1)} %add_rsqrt_fusion, bf16[128,2048]{1,0:T(8,128)(2,1)} %param.21, s32[]{:T(128)S(6)} %select_n.16, s32[128]{0:T(128)S(1)} %get-tuple-element.9, s32[128]{0:T(128)S(1)} %get-tuple-element.8), kind=kOutput, calls=%fused_computation | convolution fusion | flops 68157440 | bytes 658948 | tf_op jit(solution)/shard_map/dot_general | solution.py:283
  10.9 0.0 copy-done
  10.9 67.8 %shard_map.149 = (bf16[64,2048]{1,0:T(8,128)(2,1)}, bf16[128,512]{1,0:T(8,128)(2,1)}) custom-call(bf16[256,256]{1,0:T(8,128)(2,1)} %q_ref.1, bf16[256,256]{1,0:T(8,128)(2,1)} %k_ref.1, bf16[256,256]{1,0:T(8,128)(2,1)} %v_ref.1, bf16[256,256]{1,0:T(8,128)(2,1)} %g_ref.1, f32[256,2]{1,0:T(8,128)} %copy.37.cum_ref, f32[2,256]{1,0:T(2,128)} %bitcast.26, ...), custom_call_target="tpu_custom_call" | custom-call | tf_op jit(solution)/shard_map/pallas_call | solution.py:298
  78.7 1.7 %copy.45 = bf16[64,2048]{1,0:T(8,128)(2,1)} copy(bf16[64,2048]{1,0:T(8,128)(2,1)} %get-tuple-element.12) | data formatting | bytes 524288
  80.4 1.6 %copy.46 = bf16[128,512]{1,0:T(8,128)(2,1)} copy(bf16[128,512]{1,0:T(8,128)(2,1)} %get-tuple-element.13) | data formatting | bytes 262144
  (4 shorter events, 0.0 us)
Async XLA Ops:
  4.4 6.6 %copy-start = (f32[1,2,2,128]{3,1,2,0:T(2,128)}, f32[1,2,2,128]{3,1,2,0:T(2,128)S(1)}, u32[]{:S(2)}) copy-start(f32[1,2,2,128]{3,1,2,0:T(2,128)S(1)} %copy.42) | copy-start | bytes 6148

commit v2 on v1

v2 whole, which is shorter than its diff:
```python
import functools

import jax
import jax.numpy as jnp
from jax import lax
from jax.experimental import pallas as pl
from jax.experimental.pallas import tpu as pltpu
from jax.sharding import PartitionSpec as P

epsilon = 1e-06
CHUNKS = 2
PARTS = 2
BF = jnp.bfloat16
F32 = jnp.float32


def dot(a, b, dims=(((1,), (0,)), ((), ()))):
    return lax.dot_general(a, b, dims, preferred_element_type=F32)


def layer_kernel(
    n, cap, heads,
    q_ref, k_ref, v_ref, g_ref, ld_ref, gain_ref, tok_ref, norm_ref, ids_ref, rw_ref,
    ow_hbm, wg_hbm, wu_hbm, wd_hbm,
    mixer_ref, expert_ref,
    ow, wg, wu, wd, x, part, near, half, far, done, back,
    st, st_in, tot, tot_in, inner, ho, mx, mr1, ms, mr2,
    w_sem, disp_s, disp_r, st_s, st_r, tot_s, tot_r, fwd_s, fwd_r,
    red_s, red_r, redy_s, redy_r, mix_s, mix_r, ret_s, ret_r,
    piece_ref, hi_ref, lo_ref,
):
    i, j = lax.axis_index("ep"), lax.axis_index("tp")
    j1 = j + 1 - 2 * lax.rem(j, 2)
    j2 = lax.rem(j + 2, 4)
    j3 = lax.rem(j1 + 2, 4)
    places = (j, j1, j2, j3)
    rows = n * cap
    step = rows // CHUNKS
    width = x.shape[2]
    dim = gain_ref.shape[1]
    length = q_ref.shape[0]
    quarter = length // 4

    def shift(p):
        return (p + 1) // 2 if p % 2 else n - p // 2

    def ahead(p):
        return lax.rem(i + shift(p), n)

    def behind(p):
        return lax.rem(i + n - shift(p), n)

    def send(src, dst, ss, rs, dev):
        return pltpu.make_async_remote_copy(
            src_ref=src, dst_ref=dst, send_sem=ss, recv_sem=rs, device_id=dev,
            device_id_type=pl.DeviceIdType.MESH,
        )

    loads = [
        pltpu.make_async_copy(a, b, w_sem.at[m])
        for m, (a, b) in enumerate(((ow_hbm, ow), (wg_hbm, wg), (wu_hbm, wu), (wd_hbm, wd)))
    ]
    for c in loads:
        c.start()
    barrier = pltpu.get_barrier_semaphore()
    for d in range(1, n):
        pl.semaphore_signal(barrier, inc=1, device_id=(ahead(d), j), device_id_type=pl.DeviceIdType.MESH)
    for peer in (j1, j2):
        pl.semaphore_signal(barrier, inc=1, device_id=(i, peer), device_id_type=pl.DeviceIdType.MESH)

    tokens, top = ids_ref.shape
    lanes = -(-n // 128) * 128
    rows_f = tok_ref[...].astype(F32)
    scale = lax.rsqrt(jnp.mean(rows_f * rows_f, axis=-1, keepdims=True) + epsilon)
    mine = pl.ds(pl.multiple_of(j * width, width), width)
    normed = (tok_ref[:, mine].astype(F32) * scale * norm_ref[:, mine]).astype(BF)
    expert = lax.broadcasted_iota(jnp.int32, (tokens, lanes), 1)
    named = [ids_ref[:, t : t + 1] == expert for t in range(top)]
    strict = lax.broadcasted_iota(jnp.int32, (tokens, tokens), 0) > lax.broadcasted_iota(
        jnp.int32, (tokens, tokens), 1
    )
    held = sum(jnp.where(m, 1.0, 0.0) for m in named)
    before = dot(jnp.where(strict, 1.0, 0.0).astype(BF), held.astype(BF))
    slot = lax.broadcasted_iota(jnp.int32, (tokens, rows), 1)
    pick, comb = 0.0, 0.0
    for t in range(top):
        rank = jnp.sum(jnp.where(named[t], before, 0.0), axis=1, keepdims=True).astype(jnp.int32)
        d = ids_ref[:, t : t + 1] - i
        d = jnp.where(d < 0, d + n, d)
        place = jnp.where(d == 0, 0, jnp.where(2 * d <= n, 2 * d - 1, 2 * (n - d)))
        hit = slot == place * cap + rank
        pick = pick + jnp.where(hit, 1.0, 0.0)
        comb = comb + jnp.where(hit, rw_ref[:, t : t + 1], 0.0)
    piece = dot(pick.T.astype(BF), normed).astype(BF)
    piece_ref[...] = piece
    x[0, 0:cap, :] = piece[0:cap]
    pl.semaphore_wait(barrier, n + 1)

    sent = []
    disp = [None] * n
    for d in range(1, n):
        r = pl.ds(d * cap, cap)
        disp[d] = send(piece_ref.at[r], x.at[0, r], disp_s.at[d], disp_r.at[d], (ahead(d), j))
        disp[d].start()
        sent.append(disp[d])

    tot[...] = jnp.zeros_like(tot)
    hi = comb.astype(BF)
    hi_ref[...] = hi
    lo_ref[...] = (comb - hi.astype(F32)).astype(BF)
    causal = lax.broadcasted_iota(jnp.int32, (length, length), 0) >= lax.broadcasted_iota(
        jnp.int32, (length, length), 1
    )
    lower = jnp.where(causal, 1.0, 0.0)
    cum = [
        lax.dot_general(
            lower, jnp.broadcast_to(ld_ref[:, h : h + 1], (length, dim)), (((1,), (0,)), ((), ())),
            precision=lax.Precision.HIGHEST, preferred_element_type=F32,
        )
        for h in range(heads)
    ]

    for h in range(heads):
        c = slice(h * dim, (h + 1) * dim)
        total = cum[h][length - 1 : length, :]
        keys = k_ref[:, c].astype(F32) * jnp.exp(total - cum[h])
        st[h * dim : (h + 1) * dim, :] = dot(keys.T.astype(BF), v_ref[:, c]).astype(BF)
        tot[h : h + 1, :] = total
    st_c, tot_c = [None] * n, [None] * n
    for d in range(1, n):
        later = (lax.rem(i + d, n), j)
        st_c[d] = send(st, st_in.at[d], st_s.at[d], st_r.at[d], later)
        tot_c[d] = send(tot, tot_in.at[d], tot_s.at[d], tot_r.at[d], later)

    y_c, c0_c, c2_c = [], [], []
    small = step // PARTS
    group = n // (CHUNKS * PARTS)
    for u in range(CHUNKS * PARTS):
        r = pl.ds(u * small, small)
        y_c.append(send(x.at[0, r], x.at[2, r], fwd_s.at[u, 0], fwd_r.at[u, 0], (i, j2)))
        c0_c.append(send(x.at[0, r], x.at[1, r], fwd_s.at[u, 1], fwd_r.at[u, 1], (i, j1)))
        c2_c.append(send(x.at[2, r], x.at[3, r], fwd_s.at[u, 2], fwd_r.at[u, 2], (i, j1)))
    sent += y_c + c0_c + c2_c

    def forward(u):
        for d in range(max(1, u * group), (u + 1) * group):
            disp[d].wait_recv()
        y_c[u].start()
        c0_c[u].start()

    def relay(u):
        y_c[u].wait_recv()
        c2_c[u].start()

    for u in range(PARTS):
        forward(u)
    for d in range(1, n):
        @pl.when(i + d < n)
        def _():
            st_c[d].start()
            tot_c[d].start()

    for h in range(heads):
        c = slice(h * dim, (h + 1) * dim)
        scores = dot(q_ref[:, c], k_ref[:, c], (((1,), (1,)), ((), ()))) * dim ** (-0.5)
        spread = jnp.where(causal, cum[h][:, 0:1] - cum[h].T[0:1, :], -jnp.inf)
        inner[:, c] = dot((scores * jnp.exp(spread)).astype(BF), v_ref[:, c])

    for u in range(PARTS):
        forward(PARTS + u)
        relay(u)
    loads[0].wait()
    for c in loads[1:]:
        c.wait()

    def stripe(m):
        return pl.ds(pl.multiple_of(places[m] * quarter, quarter), quarter)

    mix_a = send(mx.at[stripe(1)], mr1.at[0], mix_s.at[0], mix_r.at[0], (i, j1))
    mix_b = send(mx.at[stripe(3)], mr1.at[1], mix_s.at[1], mix_r.at[1], (i, j1))
    mix_c = send(ms, mr2, mix_s.at[2], mix_r.at[2], (i, j2))
    sent += [mix_a, mix_b, mix_c]

    def retention():
        entering = jnp.zeros((heads * dim, dim), F32)
        for d in range(n - 1, 0, -1):
            @pl.when(i >= d)
            def _():
                st_c[d].wait_recv()
                tot_c[d].wait_recv()

            @pl.when(i < d)
            def _():
                st_in[d] = jnp.zeros(st_in.shape[1:], BF)
                tot_in[d] = jnp.zeros(tot_in.shape[1:], F32)

            decay = jnp.concatenate(
                [jnp.broadcast_to(jnp.exp(tot_in[d, h : h + 1, :]), (dim, dim)) for h in range(heads)], axis=0
            )
            entering = decay * entering + st_in[d].astype(F32)
        entering = entering.astype(BF)
        for h in range(heads):
            c = slice(h * dim, (h + 1) * dim)
            queries = (q_ref[:, c].astype(F32) * jnp.exp(cum[h])).astype(BF)
            kept = inner[:, c] + dot(queries, entering[h * dim : (h + 1) * dim, :])
            normed = kept * lax.rsqrt(jnp.mean(kept * kept, axis=-1, keepdims=True) + epsilon)
            ho[:, c] = (normed * gain_ref[h : h + 1, :] * jax.nn.silu(g_ref[:, c].astype(F32))).astype(BF)
        mx[...] = dot(ho[...], ow[...]).astype(BF)

        mix_b.start()
        mix_a.start()

    red, red_y = [], []
    for g in range(CHUNKS):
        r = pl.ds(g * step, step)
        red.append((
            send(part.at[1, r], near.at[0, r], red_s.at[g, 0], red_r.at[g, 0], (i, j1)),
            send(part.at[3, r], near.at[1, r], red_s.at[g, 1], red_r.at[g, 1], (i, j1)),
        ))
        sent += list(red[-1])
    for u in range(CHUNKS * PARTS):
        r = pl.ds(u * small, small)
        red_y.append(send(half.at[r], far.at[r], redy_s.at[u], redy_r.at[u], (i, j2)))
    sent += red_y

    def block(m):
        return pl.ds(pl.multiple_of(places[m] * width, width), width)

    def experts(g, between):
        r = pl.ds(g * step, step)
        gate, up = 0.0, 0.0
        for m in (0, 2, 1, 3):
            if m == 1:
                for u in range(g * PARTS, (g + 1) * PARTS):
                    c0_c[u].wait_recv()
                    c2_c[u].wait_recv()
            gate = gate + dot(x[m, r, :], wg[block(m), :])
            up = up + dot(x[m, r, :], wu[block(m), :])
        hidden = (jax.nn.silu(gate) * up).astype(BF)
        between()
        for m in (3, 2, 1, 0):
            part[m, r, :] = dot(hidden, wd[:, block(m)]).astype(BF)
            if m == 3:
                red[g][1].start()
            if m == 1:
                red[g][0].start()
                cross(g)

    def cross(g):
        red[g][1].wait_recv()
        for u in range(g * PARTS, (g + 1) * PARTS):
            r = pl.ds(u * small, small)
            half[r, :] = (part[2, r, :].astype(F32) + near[1, r, :].astype(F32)).astype(BF)
            red_y[u].start()

    ret = [None] * n
    for d in range(n):
        r = pl.ds(d * cap, cap)
        if d:
            ret[d] = send(done.at[r], back.at[r], ret_s.at[d], ret_r.at[d], (behind(d), j))
            sent.append(ret[d])

    def home(g):
        red[g][0].wait_recv()
        for u in range(g * PARTS, (g + 1) * PARTS):
            r = pl.ds(u * small, small)
            red_y[u].wait_recv()
            done[r, :] = (
                part[0, r, :].astype(F32) + near[0, r, :].astype(F32) + far[r, :].astype(F32)
            ).astype(BF)
            for d in range(u * group, (u + 1) * group):
                if d:
                    ret[d].start()
                else:
                    back[pl.ds(0, cap), :] = done[pl.ds(0, cap), :]

    def mix_cross():
        mix_b.wait_recv()
        ms[...] = (mx[stripe(2), :].astype(F32) + mr1[1].astype(F32)).astype(BF)
        mix_c.start()

    experts(0, lambda: None)
    for u in range(PARTS, CHUNKS * PARTS):
        relay(u)
    retention()
    for g in range(1, CHUNKS):
        experts(g, mix_cross if g == 1 else lambda: None)
        home(g - 1)
    mix_a.wait_recv()
    mix_c.wait_recv()
    mixer_ref[...] = (
        mx[stripe(0), :].astype(F32) + mr1[0].astype(F32) + mr2[...].astype(F32)
    ).astype(BF)
    home(CHUNKS - 1)
    for d in range(1, n):
        ret[d].wait_recv()
    expert_ref[...] = (dot(hi_ref[...], back[...]) + dot(lo_ref[...], back[...])).astype(BF)
    for c in sent:
        c.wait_send()
    for d in range(1, n):
        @pl.when(i + d < n)
        def _():
            st_c[d].wait_send()
            tot_c[d].wait_send()


def store_kernel(mixer, blended, mixer_out, blended_out, sem):
    copies = [
        pltpu.make_async_copy(mixer, mixer_out, sem.at[0]),
        pltpu.make_async_copy(blended, blended_out, sem.at[1]),
    ]
    for c in copies:
        c.start()
    for c in copies:
        c.wait()


def per_device(
    queries, key_rows, value_rows, out_gate, log_decay, head_gain, out_weight,
    moe_input, moe_gain, expert_gate, expert_up, expert_down, route_ids, route_weights,
):
    n, shares = lax.axis_size("ep"), lax.axis_size("tp")
    tokens, top = route_ids.shape
    pairs = tokens * top
    cap = -(-2 * pairs // n // 16) * 16
    full = moe_input.shape[1]
    width = full // shares
    length, heads = log_decay.shape
    dim = head_gain.shape[1]
    hidden = expert_gate.shape[2]

    rows = n * cap
    quarter = length // shares
    vmem = pl.BlockSpec(memory_space=pltpu.VMEM)
    hbm = pl.BlockSpec(memory_space=pltpu.HBM)
    dma = pltpu.SemaphoreType.DMA
    mixer, blended = pl.pallas_call(
        functools.partial(layer_kernel, n, cap, heads),
        out_shape=(
            jax.ShapeDtypeStruct((quarter, full), BF),
            jax.ShapeDtypeStruct((tokens, width), BF),
        ),
        in_specs=[vmem] * 10 + [hbm] * 4,
        out_specs=(vmem, vmem),
        scratch_shapes=[
            pltpu.VMEM(out_weight.shape, BF),
            pltpu.VMEM((full, hidden), BF),
            pltpu.VMEM((full, hidden), BF),
            pltpu.VMEM((hidden, full), BF),
            pltpu.VMEM((4, rows, width), BF),
            pltpu.VMEM((4, rows, width), BF),
            pltpu.VMEM((2, rows, width), BF),
            pltpu.VMEM((rows, width), BF),
            pltpu.VMEM((rows, width), BF),
            pltpu.VMEM((rows, width), BF),
            pltpu.VMEM((rows, width), BF),
            pltpu.VMEM((heads * dim, dim), BF),
            pltpu.VMEM((n, heads * dim, dim), BF),
            pltpu.VMEM((8, dim), F32),
            pltpu.VMEM((n, 8, dim), F32),
            pltpu.VMEM((length, heads * dim), F32),
            pltpu.VMEM((length, heads * dim), BF),
            pltpu.VMEM((length, full), BF),
            pltpu.VMEM((2, quarter, full), BF),
            pltpu.VMEM((quarter, full), BF),
            pltpu.VMEM((quarter, full), BF),
            dma((4,)),
            dma((n,)), dma((n,)), dma((n,)), dma((n,)), dma((n,)), dma((n,)),
            dma((CHUNKS * PARTS, 3)), dma((CHUNKS * PARTS, 3)),
            dma((CHUNKS, 2)), dma((CHUNKS, 2)),
            dma((CHUNKS * PARTS,)), dma((CHUNKS * PARTS,)),
            dma((3,)), dma((3,)),
            dma((n,)), dma((n,)),
            pltpu.VMEM((rows, width), BF),
            pltpu.VMEM((tokens, rows), BF),
            pltpu.VMEM((tokens, rows), BF),
        ],
        compiler_params=pltpu.CompilerParams(
            collective_id=0, has_side_effects=True, vmem_limit_bytes=44 * 1024 * 1024
        ),
    )(
        queries, key_rows, value_rows, out_gate, log_decay, head_gain,
        moe_input, moe_gain.reshape(1, full), route_ids, route_weights,
        out_weight, expert_gate[0], expert_up[0], expert_down[0],
    )
    return pl.pallas_call(
        store_kernel,
        out_shape=(
            jax.ShapeDtypeStruct(mixer.shape, BF),
            jax.ShapeDtypeStruct(blended.shape, BF),
        ),
        in_specs=[vmem, vmem],
        out_specs=(hbm, hbm),
        scratch_shapes=[dma((2,))],
        compiler_params=pltpu.CompilerParams(vmem_limit_bytes=4 * 1024 * 1024),
    )(mixer, blended)


def solution(mesh):
    in_specs = (
        P("ep", "tp"),
        P("ep", "tp"),
        P("ep", "tp"),
        P("ep", "tp"),
        P("ep", "tp"),
        P("tp", None),
        P("tp", None),
        P("ep", None),
        P(),
        P("ep", None, "tp"),
        P("ep", None, "tp"),
        P("ep", "tp", None),
        P("ep", None),
        P("ep", None),
    )
    out_specs = (P(("ep", "tp"), None), P("ep", "tp"))
    return jax.shard_map(
        per_device, mesh=mesh, in_specs=in_specs, out_specs=out_specs, check_vma=False
    )
```

time: 82.3 us -> 69 us (0.84)
  Pallas kernels: 67.8 us -> 54.2 us
  local copies, waits for them, and re-layouts: 7.55 us -> 13.7 us
  other arithmetic: 3.67 us -> 0 us
  matrix products: 2.26 us -> 0 us
    pallas_call x1, Pallas kernels: 67.8 us -> 53.4 us  [per_device(): pl.pallas_call(functools.partial(layer_kernel, n, cap, heads), out_shape=...]
    unnamed x6 -> x23, local copies, waits for them, and re-layouts: 4.03 us -> 13.7 us
    dot_general x2 -> x0, matrix products: 2.26 us -> none  [the longest x1 2.06 us: per_device(): piece = jnp.dot(pick, normed, preferred_element_type=F32).astype(BF)]
    reduce_sum x1 -> x0, other arithmetic: 1.23 us -> none  [per_device(): jnp.mean(rows_f * rows_f, axis=-1, keepdims=True) + epsilon]
    convert_element_type x1 -> x0, other arithmetic: 0.85 us -> none  [per_device(): lo = (comb - hi).astype(BF)]
where the time goes in v2:
time: 69 us; the launch traced here: 68.6 us
  Pallas kernels  54.2 us (79%)
  local copies, waits for them, and re-layouts  13.7 us (20%)
    pallas_call x1, Pallas kernels, per_device(): pl.pallas_call(functools.partial(layer_kernel, n, cap, heads), out_shape=...  53.4 us
    unnamed x23, local copies, waits for them, and re-layouts  13.7 us

profile of v2, /device:TPU:0, one launch (start us, length us, event | category | flops | bytes accessed | tf_op | source)
XLA Modules:
  0.0 68.6 jit_solution(5299224652979638877)
XLA Ops:
  0.6 0.8 %copy.17.ids_ref = s32[128,2]{1,0:T(8,128)S(1)} copy(s32[128,2]{0,1:T(2,128)} %param.26) | data formatting | bytes 2048 | tf_op args[12]
  1.4 0.8 %copy.18.rw_ref = f32[128,2]{1,0:T(8,128)S(1)} copy(f32[128,2]{0,1:T(2,128)} %param.27) | data formatting | bytes 2048 | tf_op args[13]
  2.2 0.8 %copy.16.ld_ref = f32[256,2]{1,0:T(8,128)S(1)} copy(f32[256,2]{0,1:T(2,128)} %param.18) | data formatting | bytes 4096 | tf_op args[4]
  3.0 0.0 copy-start
  3.0 2.0 %copy-done = bf16[1,2048,896]{2,1,0:T(8,128)(2,1)S(1)} copy-done((bf16[1,2048,896]{2,1,0:T(8,128)(2,1)S(1)}, bf16[1,2048,896]{2,1,0:T(8,128)(2,1)}, u32[]{:S(2)}) %copy-start) | copy-done | bytes 3670040
  5.1 0.0 copy-start.1
  5.1 2.0 %copy-done.1 = bf16[1,2048,896]{2,1,0:T(8,128)(2,1)S(1)} copy-done((bf16[1,2048,896]{2,1,0:T(8,128)(2,1)S(1)}, bf16[1,2048,896]{2,1,0:T(8,128)(2,1)}, u32[]{:S(2)}) %copy-start.1) | copy-done | bytes 3670040
  7.1 0.0 copy-start.2
  7.1 1.2 %copy-done.2 = bf16[256,2048]{1,0:T(8,128)(2,1)S(1)} copy-done((bf16[256,2048]{1,0:T(8,128)(2,1)S(1)}, bf16[256,2048]{1,0:T(8,128)(2,1)}, u32[]{:S(2)}) %copy-start.2) | copy-done | bytes 1048600
  8.3 0.0 copy-start.3
  8.3 1.0 %copy-done.3 = bf16[128,2048]{1,0:T(8,128)(2,1)S(1)} copy-done((bf16[128,2048]{1,0:T(8,128)(2,1)S(1)}, bf16[128,2048]{1,0:T(8,128)(2,1)}, u32[]{:S(2)}) %copy-start.3) | copy-done | bytes 524312
  9.4 0.0 copy-start.4
  9.4 0.9 %copy-done.4 = bf16[256,256]{1,0:T(8,128)(2,1)S(1)} copy-done((bf16[256,256]{1,0:T(8,128)(2,1)S(1)}, bf16[256,256]{1,0:T(8,128)(2,1)}, u32[]{:S(2)}) %copy-start.4) | copy-done | bytes 131096
  10.3 0.0 copy-start.5
  10.3 0.9 %copy-done.5 = bf16[256,256]{1,0:T(8,128)(2,1)S(1)} copy-done((bf16[256,256]{1,0:T(8,128)(2,1)S(1)}, bf16[256,256]{1,0:T(8,128)(2,1)}, u32[]{:S(2)}) %copy-start.5) | copy-done | bytes 131096
  11.2 0.0 copy-start.6
  11.2 0.9 %copy-done.6 = bf16[256,256]{1,0:T(8,128)(2,1)S(1)} copy-done((bf16[256,256]{1,0:T(8,128)(2,1)S(1)}, bf16[256,256]{1,0:T(8,128)(2,1)}, u32[]{:S(2)}) %copy-start.6) | copy-done | bytes 131096
  12.1 0.0 copy-start.7
  12.1 0.9 %copy-done.7 = bf16[256,256]{1,0:T(8,128)(2,1)S(1)} copy-done((bf16[256,256]{1,0:T(8,128)(2,1)S(1)}, bf16[256,256]{1,0:T(8,128)(2,1)}, u32[]{:S(2)}) %copy-start.7) | copy-done | bytes 131096
  13.0 0.0 copy-start.8
  13.0 0.7 %copy-done.8 = f32[2048]{0:T(1024)S(1)} copy-done((f32[2048]{0:T(1024)S(1)}, f32[2048]{0:T(1024)}, u32[]{:S(2)}) %copy-start.8) | copy-done | bytes 8216
  13.7 0.0 copy-start.9
  13.7 0.7 copy-done.9
  14.4 53.4 %shard_map.149 = (bf16[64,2048]{1,0:T(8,128)(2,1)S(1)}, bf16[128,512]{1,0:T(8,128)(2,1)S(1)}) custom-call(bf16[256,256]{1,0:T(8,128)(2,1)S(1)} %copy-done.4, bf16[256,256]{1,0:T(8,128)(2,1)S(1)} %copy-done.5, bf16[256,256]{1,0:T(8,128)(2,1)S(1)} %copy-done.6, bf16[256,256]{1,0:T(8,128)(2,1)S(1)} %copy-done.7, f32[256,2]{1,0:T(8,128)S(1)} %copy.16.ld_ref, ...), custom_call_target="tpu_custom_call" | custom-call | tf_op jit(solution)/shard_map/pallas_call | solution.py:337
  67.8 0.8 %shard_map.150 = (bf16[64,2048]{1,0:T(8,128)(2,1)}, bf16[128,512]{1,0:T(8,128)(2,1)}) custom-call(bf16[64,2048]{1,0:T(8,128)(2,1)S(1)} %get-tuple-element.4.mixer, bf16[128,512]{1,0:T(8,128)(2,1)S(1)} %get-tuple-element.5.blended), custom_call_target="tpu_custom_call" | custom-call | tf_op jit(solution)/shard_map/pallas_call | solution.py:386
Async XLA Ops:
  3.0 2.0 %copy-start = (bf16[1,2048,896]{2,1,0:T(8,128)(2,1)S(1)}, bf16[1,2048,896]{2,1,0:T(8,128)(2,1)}, u32[]{:S(2)}) copy-start(bf16[1,2048,896]{2,1,0:T(8,128)(2,1)} %param.23) | copy-start | bytes 11010052
  5.1 2.0 %copy-start.1 = (bf16[1,2048,896]{2,1,0:T(8,128)(2,1)S(1)}, bf16[1,2048,896]{2,1,0:T(8,128)(2,1)}, u32[]{:S(2)}) copy-start(bf16[1,2048,896]{2,1,0:T(8,128)(2,1)} %param.24) | copy-start | bytes 11010052
  7.1 1.2 %copy-start.2 = (bf16[256,2048]{1,0:T(8,128)(2,1)S(1)}, bf16[256,2048]{1,0:T(8,128)(2,1)}, u32[]{:S(2)}) copy-start(bf16[256,2048]{1,0:T(8,128)(2,1)} %ow_hbm.1) | copy-start | bytes 3145732
  8.3 1.0 %copy-start.3 = (bf16[128,2048]{1,0:T(8,128)(2,1)S(1)}, bf16[128,2048]{1,0:T(8,128)(2,1)}, u32[]{:S(2)}) copy-start(bf16[128,2048]{1,0:T(8,128)(2,1)} %tok_ref.1) | copy-start | bytes 1572868
  9.4 0.9 %copy-start.4 = (bf16[256,256]{1,0:T(8,128)(2,1)S(1)}, bf16[256,256]{1,0:T(8,128)(2,1)}, u32[]{:S(2)}) copy-start(bf16[256,256]{1,0:T(8,128)(2,1)} %q_ref.1) | copy-start | bytes 393220
  10.3 0.9 %copy-start.5 = (bf16[256,256]{1,0:T(8,128)(2,1)S(1)}, bf16[256,256]{1,0:T(8,128)(2,1)}, u32[]{:S(2)}) copy-start(bf16[256,256]{1,0:T(8,128)(2,1)} %k_ref.1) | copy-start | bytes 393220
  11.2 0.9 %copy-start.6 = (bf16[256,256]{1,0:T(8,128)(2,1)S(1)}, bf16[256,256]{1,0:T(8,128)(2,1)}, u32[]{:S(2)}) copy-start(bf16[256,256]{1,0:T(8,128)(2,1)} %v_ref.1) | copy-start | bytes 393220
  12.1 0.9 %copy-start.7 = (bf16[256,256]{1,0:T(8,128)(2,1)S(1)}, bf16[256,256]{1,0:T(8,128)(2,1)}, u32[]{:S(2)}) copy-start(bf16[256,256]{1,0:T(8,128)(2,1)} %g_ref.1) | copy-start | bytes 393220
  13.0 0.7 %copy-start.8 = (f32[2048]{0:T(1024)S(1)}, f32[2048]{0:T(1024)}, u32[]{:S(2)}) copy-start(f32[2048]{0:T(1024)} %param.22) | copy-start | bytes 24580
  13.7 0.7 copy-start.9
